TPU v7x, 256 devices: a whole 4x4x8 slice. The times are simulated.
256 devices in a mesh: ep: 16 (over y, x), tp: 16 (over z, core).
Axes of the slice: x: 4, y: 4, z: 8, core: 2. Of those that a mesh axis runs over, the one named last changes fastest.
Arguments:
- tokens: bfloat16 [256, 2048], P('ep', 'tp'), may hold values from -6 to 6
- key_cache: bfloat16 [256, 16, 1024, 128], P('ep', 'tp'), may hold values from -1700 to 1700
- value_cache: bfloat16 [256, 16, 1024, 128], P('ep', 'tp'), may hold values from -6 to 6
- gate_totals: float32 [256, 16, 1024], P('ep', 'tp'), as said below
- lengths: int32 [256], P('ep'), may hold values from 128 to 1024
- attn_gain: float32 [2048], replicated, may hold values from 0.1 to 1.9
- w_query: bfloat16 [2048, 2048], P(None, 'tp'), may hold values from -0.125 to 0.125
- w_key: bfloat16 [2048, 2048], P(None, 'tp'), may hold values from -0.125 to 0.125
- w_value: bfloat16 [2048, 2048], P(None, 'tp'), may hold values from -0.125 to 0.125
- w_forget: bfloat16 [2048, 16], replicated, may hold values from -0.125 to 0.125
- forget_bias: float32 [16], replicated, may hold values from -3 to 0
- w_attn_out: bfloat16 [2048, 2048], P('tp'), may hold values from -0.1875 to 0.1875
- moe_gain: float32 [2048], replicated, may hold values from 0.1 to 1.9
- group_ids: int32 [256, 1], P('ep'), may hold values from 0 to 15; in each aligned block of 16 rows (0 to 15, 16 to 31, ...) at most 2 rows name the same one
- inner_ids: int32 [256, 2], P('ep'), may hold values from 0 to 3, all different within a row
- group_prob: float32 [256], P('ep'), may hold values from 0.2 to 1
- pair_logits: float32 [256, 2], P('ep'), may hold values from -6 to 6
- w_expert_gate: bfloat16 [16, 2048, 2048], P('ep', None, 'tp'), may hold values from -0.125 to 0.125
- w_expert_up: bfloat16 [16, 2048, 2048], P('ep', None, 'tp'), may hold values from -0.125 to 0.125
- w_expert_down: bfloat16 [16, 2048, 2048], P('ep', 'tp'), may hold values from -0.375 to 0.375
- w_dense_in: bfloat16 [2048, 2048], P(None, 'tp'), may hold values from -0.125 to 0.125
- w_dense_out: bfloat16 [2048, 2048], P('tp'), may hold values from -0.1875 to 0.1875
- dense_gate: float32 [2048], P('tp'), may hold values from -2 to 2
Outputs:
- layer_output: bfloat16 [256, 2048], P('ep', 'tp')
- new_keys: bfloat16 [256, 16, 128], P('ep', 'tp')
- new_values: bfloat16 [256, 16, 128], P('ep', 'tp')
- new_gates: float32 [256, 16], P('ep', 'tp')
Inputs may be any that keep to these rules, and one draw needn't show every extreme that they name: `group_ids`: within the 16 sequences of each index of ep (aligned blocks of rows), no group is named by more than 2 sequences, a bound that some block reaches. `inner_ids`: each row names 2 different experts of its group. `gate_totals`: along positions the values of each sequence and head never rise.
All inputs are finite; a program needn't handle non-finite values.
Results may differ from a plain program's by a relative error of at most 0.011.
Values may be sent and summed in bfloat16 or wider, within the bound.
A program may use at most 64 MiB of HBM per device.

v0:
```python
import jax
import jax.numpy as jnp
from jax import lax
from jax.sharding import PartitionSpec as P

FFE = 512
EPG = 4
EPS = 1e-06
FLOOR = -1e30


def split_up(array, dim, size):
    dims = array.shape
    pieces = array.reshape(*dims[:dim], size, dims[dim] // size, *dims[dim + 1 :])
    return jnp.moveaxis(pieces, dim, 0)


def sum_at_owner(array, axis, dim):
    size = lax.axis_size(axis)
    pieces = lax.all_to_all(split_up(array, dim, size), axis, 0, 0, tiled=True)
    return jnp.sum(pieces, axis=0)


def joined_along(pieces, dim):
    dims = list(pieces.shape[1:])
    dims[dim] *= pieces.shape[0]
    return jnp.moveaxis(pieces, 0, dim).reshape(dims)


def copy_for_each(array, axis):
    copies = jnp.broadcast_to(array, (lax.axis_size(axis), *array.shape))
    return lax.all_to_all(copies, axis, split_axis=0, concat_axis=0, tiled=True)


def gathered_copies(array, axis, dim):
    return joined_along(copy_for_each(array, axis), dim)


def side_by_side(arrays, axis, split_dim, concat_dim, along):
    both = jnp.concatenate(arrays, axis=along)
    filled, at, gathered = (
        lax.all_to_all(both, axis, split_axis=split_dim, concat_axis=concat_dim, tiled=True),
        0,
        [],
    )
    for a in arrays:
        gathered.append(lax.slice_in_dim(filled, at, at + a.shape[along], axis=along))
        at += a.shape[along]
    return tuple(gathered)


def sent_together(arrays, axis, dim, along):
    widths = [a.shape[along] for a in arrays]
    both = jnp.concatenate(arrays, axis=along)
    filled = sum_at_owner(both, axis, dim)
    return tuple(jnp.split(filled, [sum(widths[:k]) for k in range(1, len(widths))], axis=along))


def norm_rows(row_data, gain_vec):
    values = row_data.astype(jnp.float32)
    factor = lax.rsqrt(jnp.mean(values * values, axis=-1, keepdims=True) + EPS)
    return (values * factor * gain_vec).astype(jnp.bfloat16)


def head_norm(values):
    factor = lax.rsqrt(jnp.mean(values * values, axis=-1, keepdims=True) + EPS)
    return (values * factor).astype(jnp.bfloat16)


def attend(queries, fresh_key, fresh_value, key_cache, value_cache, gate_totals, lengths, current):
    score_scale = queries.shape[-1] ** (-0.5)
    scores = (
        jnp.einsum("shd,shld->shl", queries, key_cache, preferred_element_type=jnp.float32)
        * score_scale
    )
    scores = scores + current[:, :, None] - gate_totals
    entry_indices = jnp.arange(key_cache.shape[2])
    live_mask = (entry_indices[None, :] < lengths[:, None])[:, None, :]
    scores = jnp.where(live_mask, scores, FLOOR)
    own_score = (
        jnp.sum(queries.astype(jnp.float32) * fresh_key.astype(jnp.float32), axis=-1) * score_scale
    )
    peak = jnp.maximum(jnp.max(scores, axis=-1), own_score)
    expo_terms = jnp.where(live_mask, jnp.exp(scores - peak[:, :, None]), 0.0)
    own_expo = jnp.exp(own_score - peak)
    denom_sum = jnp.sum(expo_terms, axis=-1) + own_expo
    weights = (expo_terms / denom_sum[:, :, None]).astype(jnp.bfloat16)
    own_weight = (own_expo / denom_sum).astype(jnp.bfloat16)
    attended = jnp.einsum("shl,shld->shd", weights, value_cache, preferred_element_type=jnp.float32)
    attended = attended + own_weight.astype(jnp.float32)[:, :, None] * fresh_value.astype(
        jnp.float32
    )
    return attended.astype(jnp.bfloat16)


def body(
    tokens,
    key_cache,
    value_cache,
    gate_totals,
    lengths,
    attn_gain,
    w_query,
    w_key,
    w_value,
    w_forget,
    forget_bias,
    w_attn_out,
    moe_gain,
    group_ids,
    inner_ids,
    group_prob,
    pair_logits,
    w_expert_gate,
    w_expert_up,
    w_expert_down,
    w_dense_in,
    w_dense_out,
    dense_gate,
):
    gathered = lax.all_gather(tokens, "tp", axis=1, tiled=True)
    normed = norm_rows(gathered, attn_gain)
    seq_count = gathered.shape[0]
    heads_dev = key_cache.shape[1]
    head_dim = key_cache.shape[3]

    def project(weight):
        return jnp.dot(normed, weight, preferred_element_type=jnp.float32).reshape(
            seq_count, heads_dev, head_dim
        )

    queries = head_norm(project(w_query))
    new_keys = head_norm(project(w_key))
    new_values = project(w_value).astype(jnp.bfloat16)
    first_head = lax.axis_index("tp") * heads_dev
    forget_cols = lax.dynamic_slice_in_dim(w_forget, first_head, heads_dev, 1)
    forget_shift = lax.dynamic_slice_in_dim(forget_bias, first_head, heads_dev, 0)
    log_gate = jax.nn.log_sigmoid(
        jnp.dot(normed, forget_cols, preferred_element_type=jnp.float32) + forget_shift
    )
    entry_indices = jnp.arange(gate_totals.shape[2])
    at_last = (entry_indices[None, :] == (lengths - 1)[:, None])[:, None, :]
    new_gates = jnp.sum(jnp.where(at_last, gate_totals, 0.0), axis=2) + log_gate
    attended = attend(
        queries, new_keys, new_values, key_cache, value_cache, gate_totals, lengths, new_gates
    )
    partial_value = jnp.dot(
        attended.reshape(seq_count, heads_dev * head_dim),
        w_attn_out,
        preferred_element_type=jnp.float32,
    )
    piece_sum = sum_at_owner(partial_value, "tp", 1)
    own_residual = (tokens.astype(jnp.float32) + piece_sum).astype(jnp.bfloat16)
    moe_in = norm_rows(gathered_copies(own_residual, "tp", 1), moe_gain)
    groups = lax.axis_size("ep")
    capacity = max(2, 2 * seq_count // groups)
    first_share = jax.nn.sigmoid(pair_logits[:, 0] - pair_logits[:, 1])
    pair_share = group_prob[:, None] * jnp.stack([first_share, 1.0 - first_share], axis=1)
    inner_range = jnp.arange(EPG)
    spread = jnp.sum(
        jnp.where(inner_ids[:, :, None] == inner_range[None, None, :], pair_share[:, :, None], 0.0),
        axis=1,
    ).astype(jnp.bfloat16)
    choose = (group_ids == jnp.arange(groups)[None, :]).astype(jnp.int32)
    before = jnp.cumsum(choose, axis=0) - choose
    slot_of = group_ids[:, 0] * capacity + jnp.sum(before * choose, axis=1)
    slot_ids = jnp.arange(groups * capacity)
    send_map = (slot_of[None, :] == slot_ids[:, None]).astype(jnp.bfloat16)
    send_weights = jnp.dot(send_map, spread, preferred_element_type=jnp.float32).astype(
        jnp.bfloat16
    )
    send_rows = jnp.dot(send_map, moe_in, preferred_element_type=jnp.float32).astype(jnp.bfloat16)
    recv_rows, recv_weights = side_by_side((send_rows, send_weights), "ep", 0, 0, 1)
    dense_hidden = jax.nn.silu(
        jnp.dot(moe_in, w_dense_in, preferred_element_type=jnp.float32)
    ).astype(jnp.bfloat16)
    dense_part = jnp.dot(dense_hidden, w_dense_out, preferred_element_type=jnp.float32)
    hidden_dev = w_expert_gate.shape[2]
    expert_index = lax.axis_index("tp") * hidden_dev // FFE
    route_col = jnp.sum(
        jnp.where(inner_range[None, :] == expert_index, recv_weights.astype(jnp.float32), 0.0),
        axis=1,
    )
    gate_pre = jnp.dot(recv_rows, w_expert_gate[0], preferred_element_type=jnp.float32)
    up_pre = jnp.dot(recv_rows, w_expert_up[0], preferred_element_type=jnp.float32)
    hidden = (jax.nn.silu(gate_pre) * up_pre * route_col[:, None]).astype(jnp.bfloat16)
    expert_part = jnp.dot(hidden, w_expert_down[0], preferred_element_type=jnp.float32)
    expert_sum, dense_sum = sent_together((expert_part, dense_part), "tp", 1, 0)
    returned = lax.all_to_all(
        expert_sum.astype(jnp.bfloat16), "ep", split_axis=0, concat_axis=0, tiled=True
    )
    expert_out = lax.dot_general(
        send_map, returned, (((0,), (0,)), ((), ())), preferred_element_type=jnp.float32
    )
    layer_output = (
        own_residual.astype(jnp.float32) + expert_out + jax.nn.sigmoid(dense_gate) * dense_sum
    )
    return (layer_output.astype(jnp.bfloat16), new_keys, new_values, new_gates)


def solution(mesh):
    placed = (
        P("ep", "tp"),
        P("ep", "tp", None, None),
        P("ep", "tp", None, None),
        P("ep", "tp", None),
        P("ep"),
        P(),
        P(None, "tp"),
        P(None, "tp"),
        P(None, "tp"),
        P(),
        P(),
        P("tp", None),
        P(),
        P("ep", None),
        P("ep", None),
        P("ep"),
        P("ep", None),
        P("ep", None, "tp"),
        P("ep", None, "tp"),
        P("ep", "tp", None),
        P(None, "tp"),
        P("tp", None),
        P("tp"),
    )
    return jax.shard_map(
        body,
        mesh=mesh,
        in_specs=placed,
        out_specs=(P("ep", "tp"), P("ep", "tp", None), P("ep", "tp", None), P("ep", "tp")),
        check_vma=False,
    )
```

profile of v0, /device:TPU:1, one launch (start us, length us, event | category | flops | bytes accessed | tf_op | source)
XLA Modules:
  0.0 108.0 jit_solution(13230268292263461012)
XLA Ops:
  0.7 21.8 %all_gather.3 = bf16[16,2048]{1,0:T(8,128)(2,1)S(1)} all-gather(bf16[16,128]{1,0:T(8,128)(2,1)} %param.23), channel_id=1, replica_groups=mesh['ep'=16,'tp'=16] {'tp'}, dimensions={1}, use_global_device_ids=true | all-gather | bytes 69632 | tf_op jit(solution)/shard_map/all_gather | solution.py:121
  22.7 1.4 %multiply_reduce_fusion.1 = (f32[16]{0:T(128)S(1)}, f32[16,128]{1,0:T(8,128)S(1)}) fusion(bf16[2048,128]{1,0:T(8,128)(2,1)} %param.30, bf16[16,2048]{1,0:T(8,128)(2,1)S(1)} %all_gather.3, f32[2048]{0:T(1024)} %param.28, f32[16]{0:T(128)S(1)} %add_rsqrt_fusion.3), kind=kOutput, calls=%fused_computation.71 | convolution fusion | flops 8523760 | bytes 606336 | tf_op jit(solution)/shard_map/dot_general | solution.py:128
  24.1 1.4 %multiply_reduce_fusion.2 = (f32[16]{0:T(128)S(1)}, f32[16,128]{1,0:T(8,128)S(1)}) fusion(bf16[2048,128]{1,0:T(8,128)(2,1)} %param.29, bf16[16,2048]{1,0:T(8,128)(2,1)S(1)} %all_gather.3, f32[2048]{0:T(1024)} %param.28, f32[16]{0:T(128)S(1)} %add_rsqrt_fusion.3), kind=kOutput, calls=%fused_computation.74 | convolution fusion | flops 8523760 | bytes 606336 | tf_op jit(solution)/shard_map/dot_general | solution.py:128
  25.5 0.7 broadcast_add_fusion
  26.2 0.8 fusion.59
  27.0 3.4 %fusion.2 = f32[16,1,1024]{2,1,0:T(1,128)S(1)} fusion(bf16[16,1,1024,128]{3,2,1,0:T(8,128)(2,1)} %param.24, bf16[16,128,1]{1,0,2:T(8,128)(2,1)S(1)} %get-tuple-element.10), kind=kOutput, calls=%fused_computation.2 | convolution fusion | flops 4194304 | bytes 4263936 | tf_op jit(solution)/shard_map/shd,shld->shl/dot_general | solution.py:73
  30.4 0.6 dynamic_slice.7
  31.3 1.6 %fusion.51 = f32[16]{0:T(128)S(1)} fusion(f32[16]{0:T(128)S(1)} %fusion.29, bf16[2048,16]{0,1:T(8,128)(2,1)} %param.32, s32[]{:T(128)S(6)} %select_n.34, f32[]{:T(128)} %bitcast.4, bf16[16,2048]{1,0:T(8,128)(2,1)S(1)} %all_gather.3, f32[2048]{0:T(1024)S(1)} %copy-done.8, f32[16]{0:T(128)S(1)} %add_rsqrt_fusion.3), kind=kOutput, calls=%fused_computation.85 | convolution fusion | flops 196768 | bytes 82628 | tf_op jit(solution)/shard_map/dot_general | solution.py:139
  34.3 3.0 %fusion = f32[16,1,128]{2,1,0:T(1,128)S(1)} fusion(bf16[16,1,1024,128]{3,2,1,0:T(8,128)(2,1)} %param.25, f32[16]{0:T(128)S(1)} %get-tuple-element.12, f32[16,1,1024]{2,1,0:T(1,128)S(1)} %get-tuple-element.7, f32[16]{0:T(128)S(1)} %multiply_maximum_fusion, s32[16]{0:T(128)S(1)} %copy-done.12), kind=kOutput, calls=%fused_computation | convolution fusion | flops 4276224 | bytes 4268224 | tf_op jit(solution)/shard_map/shl,shld->shd/dot_general | solution.py:89
  37.3 0.9 convolution_bitcast_fusion
  38.3 3.8 %all-to-all-start = ((f32[16,16,128]{2,1,0:T(8,128)}), f32[16,16,128]{2,1,0:T(8,128)S(1)}, u32[]{:S(2)}, u32[]{:S(2)}) async-start(f32[16,16,128]{2,1,0:T(8,128)} %convolution_bitcast_fusion), calls=%async_computation | async-start | bytes 262144 | tf_op jit(solution)/shard_map/all_to_all | solution.py:20
  42.5 8.5 %all-to-all-done = f32[16,16,128]{2,1,0:T(8,128)S(1)} async-done(((f32[16,16,128]{2,1,0:T(8,128)}), f32[16,16,128]{2,1,0:T(8,128)S(1)}, u32[]{:S(2)}, u32[]{:S(2)}) %all-to-all-start) | async-done | bytes 131104 | tf_op jit(solution)/shard_map/all_to_all | solution.py:20
  51.0 0.6 broadcast_in_dim.32
  51.6 3.4 %all-to-all-start.1 = ((bf16[16,16,128]{2,1,0:T(8,128)(2,1)}), bf16[16,16,128]{2,1,0:T(8,128)(2,1)S(1)}, u32[]{:S(2)}, u32[]{:S(2)}) async-start(bf16[16,16,128]{2,1,0:T(8,128)(2,1)} %broadcast_in_dim.32), calls=%async_computation.1 | async-start | bytes 131072 | tf_op jit(solution)/shard_map/all_to_all | solution.py:32
  55.3 7.2 %all-to-all-done.1 = bf16[16,16,128]{2,1,0:T(8,128)(2,1)S(1)} async-done(((bf16[16,16,128]{2,1,0:T(8,128)(2,1)}), bf16[16,16,128]{2,1,0:T(8,128)(2,1)S(1)}, u32[]{:S(2)}, u32[]{:S(2)}) %all-to-all-start.1) | async-done | bytes 65568 | tf_op jit(solution)/shard_map/all_to_all | solution.py:32
  62.9 0.7 all_to_all.27
  63.6 6.8 %all-to-all-start.2 = ((bf16[16,2,2052]{2,1,0:T(2,128)(2,1)}), bf16[16,2,2052]{2,1,0:T(2,128)(2,1)S(1)}, u32[]{:S(2)}, u32[]{:S(2)}) async-start(bf16[16,2,2052]{2,1,0:T(2,128)(2,1)} %all_to_all.27), calls=%async_computation.2 | async-start | bytes 278528 | tf_op jit(solution)/shard_map/all_to_all | solution.py:42
  70.4 0.4 fusion.44
  70.8 6.4 %all-to-all-done.2 = bf16[16,2,2052]{2,1,0:T(2,128)(2,1)S(1)} async-done(((bf16[16,2,2052]{2,1,0:T(2,128)(2,1)}), bf16[16,2,2052]{2,1,0:T(2,128)(2,1)S(1)}, u32[]{:S(2)}, u32[]{:S(2)}) %all-to-all-start.2) | async-done | bytes 131360 | tf_op jit(solution)/shard_map/all_to_all | solution.py:42
  78.1 18.6 %all_to_all.39 = f32[16,48,128]{2,1,0:T(8,128)S(1)} all-to-all(f32[16,48,128]{2,1,0:T(8,128)S(1)} %bitcast_bitcast_fusion), channel_id=1, replica_groups=mesh['ep'=16,'tp'=16] {'tp'}, dimensions={0} | all-to-all | bytes 786432 | tf_op jit(solution)/shard_map/all_to_all | solution.py:20
  96.8 0.6 split.15
  97.4 3.5 %all-to-all-start.4 = ((bf16[16,2,128]{2,1,0:T(2,128)(2,1)}), bf16[16,2,128]{2,1,0:T(2,128)(2,1)S(1)}, u32[]{:S(2)}, u32[]{:S(2)}) async-start(bf16[16,2,128]{2,1,0:T(2,128)(2,1)} %bitcast.19), calls=%async_computation.4 | async-start | bytes 16384 | tf_op jit(solution)/shard_map/all_to_all | solution.py:189
  100.9 6.3 %all-to-all-done.4 = bf16[16,2,128]{2,1,0:T(2,128)(2,1)S(1)} async-done(((bf16[16,2,128]{2,1,0:T(2,128)(2,1)}), bf16[16,2,128]{2,1,0:T(2,128)(2,1)S(1)}, u32[]{:S(2)}, u32[]{:S(2)}) %all-to-all-start.4) | async-done | bytes 8224 | tf_op jit(solution)/shard_map/all_to_all | solution.py:189
  107.3 0.8 fusion.8
  (74 shorter events, 3.7 us)
Async XLA Ops:
  0.6 77.0 %copy-start = (bf16[1,128,2048]{2,1,0:T(8,128)(2,1)S(1)}, bf16[1,128,2048]{2,1,0:T(8,128)(2,1)}, u32[]{:S(2)}) copy-start(bf16[1,128,2048]{2,1,0:T(8,128)(2,1)} %param.42) | copy-start | bytes 1572868
  0.6 30.7 %copy-start.8 = (f32[2048]{0:T(1024)S(1)}, f32[2048]{0:T(1024)}, u32[]{:S(2)}) copy-start(f32[2048]{0:T(1024)} %param.28) | copy-start | bytes 24580
  0.7 32.4 %copy-start.12 = (s32[16]{0:T(128)S(1)}, s32[16]{0:T(128)}, u32[]{:S(2)}) copy-start(s32[16]{0:T(128)} %param.27) | copy-start | bytes 196
  0.7 29.7 %copy-start.18 = (f32[16]{0:T(128)S(1)}, f32[16]{0:T(128)}, u32[]{:S(2)}) copy-start(f32[16]{0:T(128)} %param.33) | copy-start | bytes 196
  0.7 30.3 %copy-start.7 = (f32[16,1,1024]{2,1,0:T(1,128)S(1)}, f32[16,1,1024]{2,1,0:T(1,128)}, u32[]{:S(2)}) copy-start(f32[16,1,1024]{2,1,0:T(1,128)} %param.26) | copy-start | bytes 196612
  0.7 33.0 %copy-start.1 = (bf16[2048,128]{1,0:T(8,128)(2,1)S(1)}, bf16[2048,128]{1,0:T(8,128)(2,1)}, u32[]{:S(2)}) copy-start(bf16[2048,128]{1,0:T(8,128)(2,1)} %param.31) | copy-start | bytes 1572868
  0.7 33.3 %copy-start.2 = (bf16[128,2048]{1,0:T(8,128)(2,1)S(1)}, bf16[128,2048]{1,0:T(8,128)(2,1)}, u32[]{:S(2)}) copy-start(bf16[128,2048]{1,0:T(8,128)(2,1)} %param.34) | copy-start | bytes 1572868
  30.4 11.7 %copy-start.13 = (s32[16,1]{0,1:T(1,128)S(1)}, s32[16,1]{0,1:T(1,128)}, u32[]{:S(2)}) copy-start(s32[16,1]{0,1:T(1,128)} %param.36) | copy-start | bytes 196
  30.4 12.0 %copy-start.15 = (f32[16,2]{0,1:T(2,128)S(1)}, f32[16,2]{0,1:T(2,128)}, u32[]{:S(2)}) copy-start(f32[16,2]{0,1:T(2,128)} %param.39) | copy-start | bytes 388
  30.4 12.0 %copy-start.17 = (f32[16]{0:T(128)S(1)}, f32[16]{0:T(128)}, u32[]{:S(2)}) copy-start(f32[16]{0:T(128)} %param.38) | copy-start | bytes 196
  30.4 12.1 %copy-start.14 = (s32[16,2]{0,1:T(2,128)S(1)}, s32[16,2]{0,1:T(2,128)}, u32[]{:S(2)}) copy-start(s32[16,2]{0,1:T(2,128)} %param.37) | copy-start | bytes 388
  30.4 20.6 %copy-start.11 = (bf16[16,128]{1,0:T(8,128)(2,1)S(1)}, bf16[16,128]{1,0:T(8,128)(2,1)}, u32[]{:S(2)}) copy-start(bf16[16,128]{1,0:T(8,128)(2,1)} %param.23) | copy-start | bytes 12292
  30.4 32.2 %copy-start.9 = (f32[2048]{0:T(1024)S(1)}, f32[2048]{0:T(1024)}, u32[]{:S(2)}) copy-start(f32[2048]{0:T(1024)} %param.35) | copy-start | bytes 24580
  32.9 29.9 %copy-start.16 = (f32[16]{0:T(128)}, f32[16]{0:T(128)S(1)}, u32[]{:S(2)}) copy-start(f32[16]{0:T(128)S(1)} %fusion.51) | copy-start | bytes 196
  34.0 36.8 %copy-start.10 = (bf16[16,128]{1,0:T(8,128)(2,1)}, bf16[16,128]{1,0:T(8,128)(2,1)S(1)}, u32[]{:S(2)}) copy-start(bf16[16,128]{1,0:T(8,128)(2,1)S(1)} %convolution_convert_fusion.1) | copy-start | bytes 12292
  34.0 36.4 %copy-start.3 = (bf16[128,2048]{1,0:T(8,128)(2,1)S(1)}, bf16[128,2048]{1,0:T(8,128)(2,1)}, u32[]{:S(2)}) copy-start(bf16[128,2048]{1,0:T(8,128)(2,1)} %param.44) | copy-start | bytes 1572868
  34.0 36.4 %copy-start.4 = (bf16[2048,128]{1,0:T(8,128)(2,1)S(1)}, bf16[2048,128]{1,0:T(8,128)(2,1)}, u32[]{:S(2)}) copy-start(bf16[2048,128]{1,0:T(8,128)(2,1)} %param.43) | copy-start | bytes 1572868
  34.3 43.2 %copy-start.5 = (bf16[1,2048,128]{2,1,0:T(8,128)(2,1)S(1)}, bf16[1,2048,128]{2,1,0:T(8,128)(2,1)}, u32[]{:S(2)}) copy-start(bf16[1,2048,128]{2,1,0:T(8,128)(2,1)} %param.40) | copy-start | bytes 1572868
  34.3 43.4 %copy-start.6 = (bf16[1,2048,128]{2,1,0:T(8,128)(2,1)S(1)}, bf16[1,2048,128]{2,1,0:T(8,128)(2,1)}, u32[]{:S(2)}) copy-start(bf16[1,2048,128]{2,1,0:T(8,128)(2,1)} %param.41) | copy-start | bytes 1572868
  37.3 63.6 %copy-start.19 = (f32[128]{0:T(128)S(1)}, f32[128]{0:T(128)}, u32[]{:S(2)}) copy-start(f32[128]{0:T(128)} %param.45) | copy-start | bytes 1540
  38.3 12.7 %all-to-all-start = ((f32[16,16,128]{2,1,0:T(8,128)}), f32[16,16,128]{2,1,0:T(8,128)S(1)}, u32[]{:S(2)}, u32[]{:S(2)}) async-start(f32[16,16,128]{2,1,0:T(8,128)} %convolution_bitcast_fusion), calls=%async_computation | async-start | bytes 262144 | tf_op jit(solution)/shard_map/all_to_all | solution.py:20
  51.6 10.9 %all-to-all-start.1 = ((bf16[16,16,128]{2,1,0:T(8,128)(2,1)}), bf16[16,16,128]{2,1,0:T(8,128)(2,1)S(1)}, u32[]{:S(2)}, u32[]{:S(2)}) async-start(bf16[16,16,128]{2,1,0:T(8,128)(2,1)} %broadcast_in_dim.32), calls=%async_computation.1 | async-start | bytes 131072 | tf_op jit(solution)/shard_map/all_to_all | solution.py:32
  63.6 13.6 %all-to-all-start.2 = ((bf16[16,2,2052]{2,1,0:T(2,128)(2,1)}), bf16[16,2,2052]{2,1,0:T(2,128)(2,1)S(1)}, u32[]{:S(2)}, u32[]{:S(2)}) async-start(bf16[16,2,2052]{2,1,0:T(2,128)(2,1)} %all_to_all.27), calls=%async_computation.2 | async-start | bytes 278528 | tf_op jit(solution)/shard_map/all_to_all | solution.py:42
  97.4 9.9 %all-to-all-start.4 = ((bf16[16,2,128]{2,1,0:T(2,128)(2,1)}), bf16[16,2,128]{2,1,0:T(2,128)(2,1)S(1)}, u32[]{:S(2)}, u32[]{:S(2)}) async-start(bf16[16,2,128]{2,1,0:T(2,128)(2,1)} %bitcast.19), calls=%async_computation.4 | async-start | bytes 16384 | tf_op jit(solution)/shard_map/all_to_all | solution.py:189
where the time goes:
time: 109 us; the launch traced here: 108 us
  blocking collectives  40.5 us (37%)
  waiting for transfers between devices  28.5 us (26%)
  starting transfers between devices  17.4 us (16%)
  matrix products  14.1 us (13%)
  other arithmetic  3.35 us (3%)
  local copies, waits for them, and re-layouts  3.12 us (3%)
    all_gather x1, blocking collectives, body(): gathered = lax.all_gather(tokens, 'tp', axis=1, tiled=True)  21.8 us
    all_to_all x1, blocking collectives, sum_at_owner(): pieces = lax.all_to_all(split_up(array, dim, size), axis, 0, 0, tiled=True)  18.6 us
    all_to_all x1, waiting for transfers between devices, sum_at_owner(): pieces = lax.all_to_all(split_up(array, dim, size), axis, 0, 0, tiled=True)  8.5 us
    all_to_all x1, waiting for transfers between devices, copy_for_each(): return lax.all_to_all(copies, axis, split_axis=0, concat_axis=0, tiled=True)  7.21 us
    all_to_all x1, starting transfers between devices, side_by_side(): lax.all_to_all(both, axis, split_axis=split_dim, concat_axis=concat_dim,...  6.75 us
    all_to_all x1, waiting for transfers between devices, side_by_side(): lax.all_to_all(both, axis, split_axis=split_dim, concat_axis=concat_dim,...  6.44 us
    all_to_all x1, waiting for transfers between devices, body(): lax.all_to_all(expert_sum.astype(jnp.bfloat16), 'ep', split_axis=0, conca...  6.35 us
    all_to_all x1, starting transfers between devices, sum_at_owner(): pieces = lax.all_to_all(split_up(array, dim, size), axis, 0, 0, tiled=True)  3.81 us
  transfers between devices with their start and end apart: 4, of which 4 were waited for; matrix products, arithmetic and copies ran while one was open for 1% of the time, Pallas kernels for 0%

commit v1 on v0

--- a/solution.py
+++ b/solution.py
@@ -118,7 +118,11 @@
     w_dense_out,
     dense_gate,
 ):
-    gathered = lax.all_gather(tokens, "tp", axis=1, tiled=True)
+    size_2 = lax.axis_size("tp")
+    repeats = [size_2 if d == 1 else 1 for d in range(tokens.ndim)]
+    gathered = lax.all_to_all(
+        jnp.tile(tokens, repeats), "tp", split_axis=1, concat_axis=1, tiled=True
+    )
     normed = norm_rows(gathered, attn_gain)
     seq_count = gathered.shape[0]
     heads_dev = key_cache.shape[1]

time: 109 us -> 105 us (0.963)
  blocking collectives: 40.5 us -> 18.6 us
  starting transfers between devices: 17.4 us -> 30.5 us
  other arithmetic: 3.35 us -> 6.91 us
  local copies, waits for them, and re-layouts: 3.12 us -> 6.18 us
  matrix products: 14.1 us -> 12.1 us
    all_gather x1 -> x0, blocking collectives: 21.8 us -> none  [body(): gathered = lax.all_gather(tokens, 'tp', axis=1, tiled=True)]
    all_to_all x0 -> x1, starting transfers between devices: none -> 9.97 us  [body(): lax.all_to_all(jnp.tile(tokens, repeats), 'tp', split_axis=1, concat_axis...]
    all_to_all x1, starting transfers between devices: 3.81 us -> 6.86 us  [sum_at_owner(): pieces = lax.all_to_all(split_up(array, dim, size), axis, 0, 0, tiled=True)]
    dot_general x1, matrix products: 2.99 us -> 0.72 us  [attend(): jnp.einsum('shl,shld->shd', weights, value_cache, preferred_element_type=...]
    another operation x0 -> x1, local copies, waits for them, and re-layouts: none -> 1.38 us  [body(): jnp.tile(tokens, repeats)]
  transfers between devices with their start and end apart: 4 -> 5, of which waited for: 4 -> 5; matrix products, arithmetic and copies ran while one was open for 1% -> 8% of each run, Pallas kernels for 0% -> 0%
where the time goes in v1:
time: 105 us
  starting transfers between devices  30.5 us (29%)
  waiting for transfers between devices  29.2 us (28%)
  blocking collectives  18.6 us (18%)
  matrix products  12.1 us (12%)
  other arithmetic  6.91 us (7%)
  local copies, waits for them, and re-layouts  6.18 us (6%)
    all_to_all x1, blocking collectives, sum_at_owner(): pieces = lax.all_to_all(split_up(array, dim, size), axis, 0, 0, tiled=True)  18.6 us
    all_to_all x1, starting transfers between devices, body(): lax.all_to_all(jnp.tile(tokens, repeats), 'tp', split_axis=1, concat_axis...  9.97 us
    all_to_all x1, waiting for transfers between devices, sum_at_owner(): pieces = lax.all_to_all(split_up(array, dim, size), axis, 0, 0, tiled=True)  8.84 us
    all_to_all x1, waiting for transfers between devices, copy_for_each(): return lax.all_to_all(copies, axis, split_axis=0, concat_axis=0, tiled=True)  7.21 us
    all_to_all x1, starting transfers between devices, sum_at_owner(): pieces = lax.all_to_all(split_up(array, dim, size), axis, 0, 0, tiled=True)  6.86 us
    all_to_all x1, starting transfers between devices, side_by_side(): lax.all_to_all(both, axis, split_axis=split_dim, concat_axis=concat_dim,...  6.75 us
    all_to_all x1, waiting for transfers between devices, side_by_side(): lax.all_to_all(both, axis, split_axis=split_dim, concat_axis=concat_dim,...  6.44 us
    all_to_all x1, waiting for transfers between devices, body(): lax.all_to_all(expert_sum.astype(jnp.bfloat16), 'ep', split_axis=0, conca...  6.35 us
  transfers between devices with their start and end apart: 5, of which 5 were waited for; matrix products, arithmetic and copies ran while one was open for 8% of the time, Pallas kernels for 0%

profile of v1, /device:TPU:1, one launch (start us, length us, event | category | flops | bytes accessed | tf_op | source)
XLA Modules:
  0.0 104.5 jit_solution(7083762711332940347)
XLA Ops:
  0.7 1.4 %tile.2 = bf16[16,16,128]{2,0,1:T(8,128)(2,1)} broadcast(bf16[16,128]{1,0:T(8,128)(2,1)} %param.23), dimensions={0,2} | broadcast | bytes 69632 | tf_op jit(solution)/shard_map/tile | solution.py:124
  2.1 10.0 %all-to-all-start = ((bf16[16,16,128]{2,0,1:T(8,128)(2,1)}), bf16[16,16,128]{2,0,1:T(8,128)(2,1)S(1)}, u32[]{:S(2)}, u32[]{:S(2)}) async-start(bf16[16,16,128]{2,0,1:T(8,128)(2,1)} %tile.2), calls=%async_computation | async-start | bytes 131072 | tf_op jit(solution)/shard_map/all_to_all | solution.py:123
  12.7 1.3 %copy.65 = bf16[2048,128]{1,0:T(8,128)(2,1)S(1)} copy(bf16[2048,128]{0,1:T(8,128)(2,1)} %bitcast.127) | data formatting | bytes 1048576 | tf_op jit(solution)/shard_map/dot_general | solution.py:151
  14.0 0.7 fusion.47
  14.8 0.8 select_reduce_fusion.1
  15.6 0.8 broadcast_subtract_fusion
  16.4 1.2 %dynamic_slice.7 = f32[1]{0:T(128)} dynamic-slice(f32[16]{0:T(128)} %param.33, s32[]{:T(128)S(6)} %select_n.34), dynamic_slice_sizes={1} | dynamic-slice | bytes 12 | tf_op jit(solution)/shard_map/dynamic_slice | solution.py:141
  18.3 1.1 %fusion.34 = f32[16]{0:T(128)S(1)} fusion(f32[16,1,1024]{2,1,0:T(1,128)} %param.26, s32[16]{0:T(128)S(1)} %broadcast_add_fusion), kind=kLoop, calls=%fused_computation.53 | loop fusion | flops 49136 | bytes 65664 | tf_op jit(solution)/shard_map/reduce_sum | solution.py:147
  19.9 1.6 %multiply_reduce_fusion.1 = (f32[16]{0:T(128)S(1)}, f32[16,128]{1,0:T(8,128)S(1)}) fusion(bf16[2048,128]{1,0:T(8,128)(2,1)} %param.30, f32[2048]{0:T(1024)} %param.28, f32[16]{0:T(128)S(1)} %add_rsqrt_fusion.3, bf16[16,16,128]{2,0,1:T(8,128)(2,1)S(1)} %all-to-all-done), kind=kOutput, calls=%fused_computation.78 | convolution fusion | flops 8523760 | bytes 606336 | tf_op jit(solution)/shard_map/dot_general | solution.py:132
  21.5 1.4 %multiply_reduce_fusion.2 = (f32[16]{0:T(128)S(1)}, f32[16,128]{1,0:T(8,128)S(1)}) fusion(bf16[2048,128]{1,0:T(8,128)(2,1)} %param.29, f32[2048]{0:T(1024)} %param.28, f32[16]{0:T(128)S(1)} %add_rsqrt_fusion.3, bf16[16,16,128]{2,0,1:T(8,128)(2,1)S(1)} %all-to-all-done), kind=kOutput, calls=%fused_computation.81 | convolution fusion | flops 8523760 | bytes 606336 | tf_op jit(solution)/shard_map/dot_general | solution.py:132
  22.9 0.8 fusion.66
  23.7 3.4 %fusion.2 = f32[16,1,1024]{2,1,0:T(1,128)S(1)} fusion(bf16[16,1,1024,128]{3,2,1,0:T(8,128)(2,1)} %param.24, bf16[16,128,1]{1,0,2:T(8,128)(2,1)S(1)} %get-tuple-element.10), kind=kOutput, calls=%fused_computation.2 | convolution fusion | flops 4194304 | bytes 4263936 | tf_op jit(solution)/shard_map/shd,shld->shl/dot_general | solution.py:73
  27.2 1.7 %fusion.56 = f32[16]{0:T(128)S(1)} fusion(f32[16]{0:T(128)S(1)} %fusion.34, bf16[2048,16]{0,1:T(8,128)(2,1)} %param.32, s32[]{:T(128)S(6)} %select_n.34, f32[]{:T(128)} %bitcast.5, bf16[16,16,128]{2,0,1:T(8,128)(2,1)S(1)} %all-to-all-done, f32[16,128]{1,0:T(8,128)S(1)} %bitcast.128, f32[16]{0:T(128)S(1)} %add_rsqrt_fusion.3), kind=kOutput, calls=%fused_computation.92 | convolution fusion | flops 196768 | bytes 82628 | tf_op jit(solution)/shard_map/dot_general | solution.py:143
  30.7 0.9 convolution_bitcast_fusion
  31.7 6.9 %all-to-all-start.1 = ((f32[16,16,128]{2,1,0:T(8,128)}), f32[16,16,128]{2,1,0:T(8,128)S(1)}, u32[]{:S(2)}, u32[]{:S(2)}) async-start(f32[16,16,128]{2,1,0:T(8,128)} %convolution_bitcast_fusion), calls=%async_computation.1 | async-start | bytes 262144 | tf_op jit(solution)/shard_map/all_to_all | solution.py:20
  38.6 8.8 %all-to-all-done.1 = f32[16,16,128]{2,1,0:T(8,128)S(1)} async-done(((f32[16,16,128]{2,1,0:T(8,128)}), f32[16,16,128]{2,1,0:T(8,128)S(1)}, u32[]{:S(2)}, u32[]{:S(2)}) %all-to-all-start.1) | async-done | bytes 131104 | tf_op jit(solution)/shard_map/all_to_all | solution.py:20
  48.1 3.4 %all-to-all-start.2 = ((bf16[16,16,128]{2,1,0:T(8,128)(2,1)}), bf16[16,16,128]{2,1,0:T(8,128)(2,1)S(1)}, u32[]{:S(2)}, u32[]{:S(2)}) async-start(bf16[16,16,128]{2,1,0:T(8,128)(2,1)} %broadcast_in_dim.32), calls=%async_computation.2 | async-start | bytes 131072 | tf_op jit(solution)/shard_map/all_to_all | solution.py:32
  51.7 7.2 %all-to-all-done.2 = bf16[16,16,128]{2,1,0:T(8,128)(2,1)S(1)} async-done(((bf16[16,16,128]{2,1,0:T(8,128)(2,1)}), bf16[16,16,128]{2,1,0:T(8,128)(2,1)S(1)}, u32[]{:S(2)}, u32[]{:S(2)}) %all-to-all-start.2) | async-done | bytes 65568 | tf_op jit(solution)/shard_map/all_to_all | solution.py:32
  60.0 6.8 %all-to-all-start.3 = ((bf16[16,2,2052]{2,1,0:T(2,128)(2,1)}), bf16[16,2,2052]{2,1,0:T(2,128)(2,1)S(1)}, u32[]{:S(2)}, u32[]{:S(2)}) async-start(bf16[16,2,2052]{2,1,0:T(2,128)(2,1)} %all_to_all.32), calls=%async_computation.3 | async-start | bytes 278528 | tf_op jit(solution)/shard_map/all_to_all | solution.py:42
  67.3 6.4 %all-to-all-done.3 = bf16[16,2,2052]{2,1,0:T(2,128)(2,1)S(1)} async-done(((bf16[16,2,2052]{2,1,0:T(2,128)(2,1)}), bf16[16,2,2052]{2,1,0:T(2,128)(2,1)S(1)}, u32[]{:S(2)}, u32[]{:S(2)}) %all-to-all-start.3) | async-done | bytes 131360 | tf_op jit(solution)/shard_map/all_to_all | solution.py:42
  74.6 18.6 %all_to_all.45 = f32[16,48,128]{2,1,0:T(8,128)S(1)} all-to-all(f32[16,48,128]{2,1,0:T(8,128)S(1)} %bitcast_bitcast_fusion), channel_id=1, replica_groups=mesh['ep'=16,'tp'=16] {'tp'}, dimensions={0} | all-to-all | bytes 786432 | tf_op jit(solution)/shard_map/all_to_all | solution.py:20
  93.8 3.5 %all-to-all-start.5 = ((bf16[16,2,128]{2,1,0:T(2,128)(2,1)}), bf16[16,2,128]{2,1,0:T(2,128)(2,1)S(1)}, u32[]{:S(2)}, u32[]{:S(2)}) async-start(bf16[16,2,128]{2,1,0:T(2,128)(2,1)} %bitcast.20), calls=%async_computation.5 | async-start | bytes 16384 | tf_op jit(solution)/shard_map/all_to_all | solution.py:193
  97.4 6.3 %all-to-all-done.5 = bf16[16,2,128]{2,1,0:T(2,128)(2,1)S(1)} async-done(((bf16[16,2,128]{2,1,0:T(2,128)(2,1)}), bf16[16,2,128]{2,1,0:T(2,128)(2,1)S(1)}, u32[]{:S(2)}, u32[]{:S(2)}) %all-to-all-start.5) | async-done | bytes 8224 | tf_op jit(solution)/shard_map/all_to_all | solution.py:193
  103.7 0.8 fusion.8
  (70 shorter events, 7.6 us)
Async XLA Ops:
  0.6 73.5 %copy-start = (bf16[1,128,2048]{2,1,0:T(8,128)(2,1)S(1)}, bf16[1,128,2048]{2,1,0:T(8,128)(2,1)}, u32[]{:S(2)}) copy-start(bf16[1,128,2048]{2,1,0:T(8,128)(2,1)} %param.42) | copy-start | bytes 1572868
  0.6 28.4 %copy-start.11 = (s32[16]{0:T(128)S(1)}, s32[16]{0:T(128)}, u32[]{:S(2)}) copy-start(s32[16]{0:T(128)} %param.27) | copy-start | bytes 196
  0.7 28.4 %copy-start.6 = (f32[16,1,1024]{2,1,0:T(1,128)S(1)}, f32[16,1,1024]{2,1,0:T(1,128)}, u32[]{:S(2)}) copy-start(f32[16,1,1024]{2,1,0:T(1,128)} %param.26) | copy-start | bytes 196612
  0.7 26.5 %copy-start.7 = (f32[2048]{0:T(1024)S(1)}, f32[2048]{0:T(1024)}, u32[]{:S(2)}) copy-start(f32[2048]{0:T(1024)} %param.28) | copy-start | bytes 24580
  2.1 17.7 %all-to-all-start = ((bf16[16,16,128]{2,0,1:T(8,128)(2,1)}), bf16[16,16,128]{2,0,1:T(8,128)(2,1)S(1)}, u32[]{:S(2)}, u32[]{:S(2)}) async-start(bf16[16,16,128]{2,0,1:T(8,128)(2,1)} %tile.2), calls=%async_computation | async-start | bytes 131072 | tf_op jit(solution)/shard_map/all_to_all | solution.py:123
  19.8 9.9 %copy-start.15 = (bf16[16,1,1024,128]{3,2,1,0:T(8,128)(2,1)S(1)}, bf16[16,1,1024,128]{3,2,1,0:T(8,128)(2,1)}, u32[]{:S(2)}) copy-start(bf16[16,1,1024,128]{3,2,1,0:T(8,128)(2,1)} %param.25) | copy-start | bytes 12582916
  23.7 6.8 %copy-start.1 = (bf16[2048,128]{1,0:T(8,128)(2,1)S(1)}, bf16[2048,128]{1,0:T(8,128)(2,1)}, u32[]{:S(2)}) copy-start(bf16[2048,128]{1,0:T(8,128)(2,1)} %param.31) | copy-start | bytes 1572868
  27.2 11.4 %copy-start.13 = (s32[16,2]{0,1:T(2,128)S(1)}, s32[16,2]{0,1:T(2,128)}, u32[]{:S(2)}) copy-start(s32[16,2]{0,1:T(2,128)} %param.37) | copy-start | bytes 388
  27.2 11.4 %copy-start.12 = (s32[16,1]{0,1:T(1,128)S(1)}, s32[16,1]{0,1:T(1,128)}, u32[]{:S(2)}) copy-start(s32[16,1]{0,1:T(1,128)} %param.36) | copy-start | bytes 196
  27.2 20.3 %copy-start.10 = (bf16[16,128]{1,0:T(8,128)(2,1)S(1)}, bf16[16,128]{1,0:T(8,128)(2,1)}, u32[]{:S(2)}) copy-start(bf16[16,128]{1,0:T(8,128)(2,1)} %param.23) | copy-start | bytes 12292
  27.2 31.9 %copy-start.8 = (f32[2048]{0:T(1024)S(1)}, f32[2048]{0:T(1024)}, u32[]{:S(2)}) copy-start(f32[2048]{0:T(1024)} %param.35) | copy-start | bytes 24580
  27.2 39.6 %copy-start.2 = (bf16[128,2048]{1,0:T(8,128)(2,1)S(1)}, bf16[128,2048]{1,0:T(8,128)(2,1)}, u32[]{:S(2)}) copy-start(bf16[128,2048]{1,0:T(8,128)(2,1)} %param.44) | copy-start | bytes 1572868
  27.2 39.6 %copy-start.3 = (bf16[2048,128]{1,0:T(8,128)(2,1)S(1)}, bf16[2048,128]{1,0:T(8,128)(2,1)}, u32[]{:S(2)}) copy-start(bf16[2048,128]{1,0:T(8,128)(2,1)} %param.43) | copy-start | bytes 1572868
  28.9 38.3 %copy-start.14 = (f32[16]{0:T(128)}, f32[16]{0:T(128)S(1)}, u32[]{:S(2)}) copy-start(f32[16]{0:T(128)S(1)} %fusion.56) | copy-start | bytes 196
  29.7 44.2 %copy-start.4 = (bf16[1,2048,128]{2,1,0:T(8,128)(2,1)S(1)}, bf16[1,2048,128]{2,1,0:T(8,128)(2,1)}, u32[]{:S(2)}) copy-start(bf16[1,2048,128]{2,1,0:T(8,128)(2,1)} %param.40) | copy-start | bytes 1572868
  29.7 44.4 %copy-start.5 = (bf16[1,2048,128]{2,1,0:T(8,128)(2,1)S(1)}, bf16[1,2048,128]{2,1,0:T(8,128)(2,1)}, u32[]{:S(2)}) copy-start(bf16[1,2048,128]{2,1,0:T(8,128)(2,1)} %param.41) | copy-start | bytes 1572868
  30.7 73.8 %copy-start.9 = (bf16[16,128]{1,0:T(8,128)(2,1)}, bf16[16,128]{1,0:T(8,128)(2,1)S(1)}, u32[]{:S(2)}) copy-start(bf16[16,128]{1,0:T(8,128)(2,1)S(1)} %convolution_convert_fusion.1) | copy-start | bytes 12292
  30.7 66.6 %copy-start.16 = (f32[128]{0:T(128)S(1)}, f32[128]{0:T(128)}, u32[]{:S(2)}) copy-start(f32[128]{0:T(128)} %param.45) | copy-start | bytes 1540
  31.7 15.7 %all-to-all-start.1 = ((f32[16,16,128]{2,1,0:T(8,128)}), f32[16,16,128]{2,1,0:T(8,128)S(1)}, u32[]{:S(2)}, u32[]{:S(2)}) async-start(f32[16,16,128]{2,1,0:T(8,128)} %convolution_bitcast_fusion), calls=%async_computation.1 | async-start | bytes 262144 | tf_op jit(solution)/shard_map/all_to_all | solution.py:20
  48.1 10.9 %all-to-all-start.2 = ((bf16[16,16,128]{2,1,0:T(8,128)(2,1)}), bf16[16,16,128]{2,1,0:T(8,128)(2,1)S(1)}, u32[]{:S(2)}, u32[]{:S(2)}) async-start(bf16[16,16,128]{2,1,0:T(8,128)(2,1)} %broadcast_in_dim.32), calls=%async_computation.2 | async-start | bytes 131072 | tf_op jit(solution)/shard_map/all_to_all | solution.py:32
  60.0 13.6 %all-to-all-start.3 = ((bf16[16,2,2052]{2,1,0:T(2,128)(2,1)}), bf16[16,2,2052]{2,1,0:T(2,128)(2,1)S(1)}, u32[]{:S(2)}, u32[]{:S(2)}) async-start(bf16[16,2,2052]{2,1,0:T(2,128)(2,1)} %all_to_all.32), calls=%async_computation.3 | async-start | bytes 278528 | tf_op jit(solution)/shard_map/all_to_all | solution.py:42
  93.8 9.9 %all-to-all-start.5 = ((bf16[16,2,128]{2,1,0:T(2,128)(2,1)}), bf16[16,2,128]{2,1,0:T(2,128)(2,1)S(1)}, u32[]{:S(2)}, u32[]{:S(2)}) async-start(bf16[16,2,128]{2,1,0:T(2,128)(2,1)} %bitcast.20), calls=%async_computation.5 | async-start | bytes 16384 | tf_op jit(solution)/shard_map/all_to_all | solution.py:193
